TPU v7x, 128 devices: a whole 4x4x4 slice. The times are simulated.
128 devices in a mesh: sp: 64 (over z, y, x), tp: 2 (over core).
Axes of the slice: x: 4, y: 4, z: 4, core: 2. Of those that a mesh axis runs over, the one named last changes fastest.
Arguments:
- input_activity: bfloat16 [8, 4096, 1024], P(None, ('sp', 'tp')), may hold values from -6 to 6
- norm_gain: bfloat16 [1024], replicated, may hold values from 0.75 to 1.25
- w_query: bfloat16 [1024, 256], P(None, 'tp'), may hold values from -0.1875 to 0.1875
- w_key: bfloat16 [1024, 256], P(None, 'tp'), may hold values from -0.1875 to 0.1875
- w_value: bfloat16 [1024, 512], P(None, 'tp'), may hold values from -0.1875 to 0.1875
- w_gate: bfloat16 [1024, 512], P(None, 'tp'), may hold values from -0.1875 to 0.1875
- head_gain: bfloat16 [4, 128], P('tp'), may hold values from 0.75 to 1.25
- w_out: bfloat16 [512, 1024], P('tp'), may hold values from -0.25 to 0.25
- initial_state: float32 [8, 4, 64, 128], P(None, 'tp'), may hold values from -48 to 48
Outputs:
- output: bfloat16 [8, 4096, 1024], P(None, ('sp', 'tp'))
- closing_memory: float32 [8, 4, 64, 128], P(None, 'tp')
All inputs are finite; a program needn't handle non-finite values.
Results may differ from a plain program's by a relative error of at most 0.015.
Values may be sent and summed in bfloat16 or wider, within the bound.
A program may use at most 64 MiB of HBM per device.

v0:
```python
import jax
import jax.numpy as jnp
from jax import lax
from jax.sharding import Mesh
from jax.sharding import PartitionSpec as P

SP = ("sp_0", "sp_1", "sp_2")
SP_TP = ("sp_0", "sp_1", "sp_2", "tp")


EPS = 1e-06
ROPE_BASE = 10000.0


def joined_along(parts, dim):
    lengths = list(parts.shape[1:])
    lengths[dim] *= parts.shape[0]
    return jnp.moveaxis(parts, 0, dim).reshape(lengths)


def on_gathered_pieces(x, axis, dim, work, out_dim):
    width = x.shape[dim]
    pieces = jnp.split(x, 2, axis=dim) if width % 2 == 0 else [x]
    first = jnp.arange(lax.axis_size(axis)) * width
    parts = [lax.all_gather(slab, axis) for slab in pieces]
    made = [jax.vmap(work)(b, first + k * (width // len(pieces))) for k, b in enumerate(parts)]
    return joined_along(jnp.concatenate(made, axis=out_dim + 1), out_dim)


def neutral_like(x, identity):
    return jax.tree.map(
        lambda part, zero: jnp.zeros_like(part) + jnp.asarray(zero, part.dtype), x, identity
    )


def entering(x, axes, combine, identity, reverse):
    before = start = neutral_like(x, identity)
    so_far = x
    for axis in reversed(axes):
        length, position = lax.axis_size(axis), lax.axis_index(axis)
        pieces = jax.tree.map(lambda part: lax.all_gather(part, axis), so_far)
        inside, so_far = start, start
        for k in reversed(range(length)) if reverse else range(length):
            passed = k > position if reverse else k < position
            so_far = combine(so_far, jax.tree.map(lambda part: part[k], pieces))
            inside = jax.tree.map(lambda new, old: jnp.where(passed, new, old), so_far, inside)
        before = combine(inside, before)
    return before


def scattered(product, width, axis):
    everything = product(jnp.int32(0), lax.axis_size(axis) * width)
    own = lax.psum_scatter(everything.astype(jnp.bfloat16), axis, scatter_dimension=0, tiled=True)
    return own.astype(jnp.float32)


def rotate(values_in, places):
    size_last = values_in.shape[-1]
    half = size_last // 2
    freqs = ROPE_BASE ** (-jnp.arange(0, size_last, 2, dtype=jnp.float32) / size_last)
    angle = places[:, None] * freqs[None, :]
    cosine = jnp.cos(angle)[None, :, None, :]
    sine = jnp.sin(angle)[None, :, None, :]
    first = values_in[..., :half]
    second = values_in[..., half:]
    return jnp.concatenate(
        [first * cosine - second * sine, first * sine + second * cosine], axis=-1
    )


def combine(earlier, later):
    return (earlier[0] * later[0], earlier[1] * later[0][None, :, None, None] + later[1])


def per_device(
    input_activity, norm_gain, w_query, w_key, w_value, w_gate, head_gain, w_out, initial_state
):
    seq_count, half_rows, model_width = input_activity.shape
    stretch = half_rows * lax.axis_size("tp")
    local_heads = initial_state.shape[1]
    key_dim = initial_state.shape[2]
    value_dim = initial_state.shape[3]
    floats = input_activity.astype(jnp.float32)
    scaled_unit = (
        floats
        * lax.rsqrt(jnp.mean(floats * floats, axis=-1, keepdims=True) + EPS)
        * norm_gain.astype(jnp.float32)
    ).astype(jnp.bfloat16)
    glued_together = jnp.concatenate([w_query, w_key, w_value, w_gate], axis=1)

    def project(segment_slice, start):
        return jnp.einsum(
            "nqe,ef->nqf", segment_slice, glued_together, preferred_element_type=jnp.float32
        ).astype(jnp.bfloat16)

    projected = on_gathered_pieces(scaled_unit, "tp", 1, project, 1)
    key_cols = local_heads * key_dim
    value_cols = local_heads * value_dim
    queries = projected[..., :key_cols].reshape(seq_count, stretch, local_heads, key_dim)
    keys_all = projected[..., key_cols : 2 * key_cols].reshape(
        seq_count, stretch, local_heads, key_dim
    )
    values_all = projected[..., 2 * key_cols : 2 * key_cols + value_cols].reshape(
        seq_count, stretch, local_heads, value_dim
    )
    gates = projected[..., 2 * key_cols + value_cols :].reshape(
        seq_count, stretch, local_heads, value_dim
    )
    places = (lax.axis_index(SP) * stretch + jnp.arange(stretch)).astype(jnp.float32)
    rot_query = rotate(queries.astype(jnp.float32), places).astype(jnp.bfloat16)
    rot_key = (rotate(keys_all.astype(jnp.float32), places) * key_dim ** (-0.5)).astype(
        jnp.bfloat16
    )
    head_ids = (lax.axis_index("tp") * local_heads + jnp.arange(local_heads)).astype(jnp.float32)
    total_len = stretch * lax.axis_size(SP)
    log_decay = -(0.25 + 0.25 * head_ids) / total_len
    steps_idx = jnp.arange(stretch, dtype=jnp.float32)
    start_positions = steps_idx[:, None] - steps_idx[None, :]
    mask = jnp.where(
        start_positions[None] >= 0,
        jnp.exp(jnp.maximum(start_positions, 0.0)[None] * log_decay[:, None, None]),
        0.0,
    )
    key_decay = jnp.exp((stretch - 1 - steps_idx)[None, :] * log_decay[:, None])
    query_decay = jnp.exp((steps_idx + 1.0)[None, :] * log_decay[:, None])
    block_decay = jnp.exp(stretch * log_decay)
    weighted_key = (rot_key.astype(jnp.float32) * key_decay.T[None, :, :, None]).astype(
        jnp.bfloat16
    )
    local_state = jnp.einsum(
        "schd,sche->shde", weighted_key, values_all, preferred_element_type=jnp.float32
    )
    identity = (jnp.ones_like(block_decay), jnp.zeros_like(local_state))
    prefix_decay, earlier_memory = entering(
        (block_decay, local_state), SP, combine, identity, False
    )
    incoming = earlier_memory + prefix_decay[None, :, None, None] * initial_state
    scores = (
        jnp.einsum("schd,skhd->shck", rot_query, rot_key, preferred_element_type=jnp.float32)
        * mask[None]
    )
    inner = jnp.einsum(
        "shck,skhe->sche",
        scores.astype(jnp.bfloat16),
        values_all,
        preferred_element_type=jnp.float32,
    )
    scaled_query = rot_query.astype(jnp.float32) * query_decay.T[None, :, :, None]
    cross = jnp.einsum("schd,shde->sche", scaled_query, incoming, precision=lax.Precision.HIGHEST)
    retained = inner + cross
    centre = jnp.mean(retained, axis=-1, keepdims=True)
    spread = jnp.mean(jnp.square(retained - centre), axis=-1, keepdims=True)
    normalized = (
        (retained - centre) * lax.rsqrt(spread + EPS) * head_gain.astype(jnp.float32)[None, None]
    )
    mixed = (
        (jax.nn.silu(gates.astype(jnp.float32)) * normalized)
        .astype(jnp.bfloat16)
        .reshape(seq_count, stretch, value_cols)
    )
    token_major = mixed.transpose(1, 0, 2)

    def output_rows(start, count):
        rows_here = lax.dynamic_slice_in_dim(token_major, start, count, 0)
        return jnp.einsum("bsm,md->bsd", rows_here, w_out, preferred_element_type=jnp.float32)

    summed = scattered(output_rows, half_rows, "tp")
    output = summed.astype(jnp.bfloat16).transpose(1, 0, 2)
    remaining = (lax.axis_size(SP) - 1 - lax.axis_index(SP)).astype(jnp.float32)
    factor = jnp.exp(log_decay * stretch * remaining)
    total = lax.psum(local_state * factor[None, :, None, None], SP)
    closing_memory = total + initial_state * jnp.exp(log_decay * total_len)[None, :, None, None]
    return (output, closing_memory)


def solution(mesh):
    split = Mesh(mesh.devices.reshape(4, 4, 4, mesh.shape["tp"]), ("sp_0", "sp_1", "sp_2", "tp"))
    placed = (
        P(None, SP_TP, None),
        P(),
        P(None, "tp"),
        P(None, "tp"),
        P(None, "tp"),
        P(None, "tp"),
        P("tp", None),
        P("tp", None),
        P(None, "tp", None, None),
    )
    return jax.shard_map(
        per_device,
        mesh=split,
        in_specs=placed,
        out_specs=(P(None, SP_TP, None), P(None, "tp", None, None)),
        check_vma=False,
    )
```

profile of v0, /device:TPU:1, one launch (start us, length us, event | category | flops | bytes accessed | tf_op | source)
XLA Modules:
  0.0 242.9 jit_solution(9718455479722213454)
XLA Ops:
  8.1 0.7 convert_element_type.98
  8.8 1.3 fusion.3
  10.2 1.2 fusion.5
  11.5 3.2 %all-gather.1 = bf16[16,16,1024]{2,1,0:T(8,128)(2,1)S(1)} all-gather(bf16[8,16,1024]{2,1,0:T(8,128)(2,1)S(1)} %get-tuple-element.24), channel_id=3, replica_groups=mesh['sp_0'=4,'sp_1'=4,'sp_2'=4,'tp'=2] {'tp'}, dimensions={0}, use_global_device_ids=true | all-gather | bytes 786432 | tf_op jit(solution)/shard_map/all_gather | solution.py:25
  14.6 2.2 all-gather
  16.8 0.6 convolution_convert_fusion.1
  17.4 0.6 convolution_convert_fusion.2
  19.0 1.2 fusion.117
  21.0 1.3 broadcast_multiply_fusion
  22.4 7.9 %all-gather.3 = f32[4,1,2]{2,1,0:T(1,128)S(1)} all-gather(f32[1,1,2]{2,1,0:T(1,128)S(1)} %exponential_bitcast_fusion), channel_id=1, replica_groups=mesh['sp_0'=4,'sp_1'=4,'sp_2'=4,'tp'=2] {'sp_2'}, dimensions={0}, use_global_device_ids=true | all-gather | bytes 40 | tf_op jit(solution)/shard_map/all_gather | solution.py:41
  30.3 24.8 %all-gather.14.cloned.1.call-done = f32[32,2,64,128]{3,2,1,0:T(8,128)} async-done(((f32[8,2,64,128]{3,2,1,0:T(8,128)}), f32[32,2,64,128]{3,2,1,0:T(8,128)}) %all-gather.14.cloned.1.call-update) | async-done | bytes 2097168 | tf_op jit(solution)/shard_map/all_gather | solution.py:41
  55.1 2.6 %bitcast_add_fusion.4 = f32[1,8,2,64,128]{4,3,2,1,0:T(8,128)} fusion(f32[32,2,64,128]{3,2,1,0:T(8,128)} %all-gather.14.cloned.1.call-done, f32[2]{0:T(128)S(1)} %get-tuple-element.35, f32[2]{0:T(128)S(1)} %get-tuple-element.36, f32[2]{0:T(128)S(1)} %get-tuple-element.37, f32[2]{0:T(128)S(1)} %bitcast_multiply_fusion.2), kind=kLoop, calls=%fused_computation.44 | loop fusion | flops 917504 | bytes 2621472 | tf_op jit(solution)/shard_map/add | solution.py:72
  57.7 7.7 %all-gather.4 = f32[4,1,2]{2,1,0:T(1,128)S(1)} all-gather(f32[1,1,2]{2,1,0:T(1,128)S(1)} %get-tuple-element.34), channel_id=1, replica_groups=mesh['sp_0'=4,'sp_1'=4,'sp_2'=4,'tp'=2] {'sp_1'}, dimensions={0}, use_global_device_ids=true | all-gather | bytes 40 | tf_op jit(solution)/shard_map/all_gather | solution.py:41
  65.4 23.1 %all-gather.10.cloned.1.call-done = f32[4,8,2,64,128]{4,3,2,1,0:T(8,128)} async-done(((f32[1,8,2,64,128]{4,3,2,1,0:T(8,128)}), f32[4,8,2,64,128]{4,3,2,1,0:T(8,128)}) %all-gather.10.cloned.1.call-update) | async-done | bytes 2097168 | tf_op jit(solution)/shard_map/all_gather | solution.py:41
  88.5 2.6 %multiply_add_fusion.1 = f32[1,8,2,64,128]{4,3,2,1,0:T(8,128)} fusion(f32[4,8,2,64,128]{4,3,2,1,0:T(8,128)} %all-gather.10.cloned.1.call-done, f32[2]{0:T(128)S(1)} %get-tuple-element.31, f32[2]{0:T(128)S(1)} %get-tuple-element.32, f32[2]{0:T(128)S(1)} %get-tuple-element.33, f32[2]{0:T(128)S(1)} %bitcast_multiply_fusion.4), kind=kLoop, calls=%fused_computation.80 | loop fusion | flops 917504 | bytes 2621472 | tf_op jit(solution)/shard_map/add | solution.py:72
  91.2 0.5 all-reduce.2.cloned.1.call-update
  91.8 7.9 %all-gather.5 = f32[4,1,2]{2,1,0:T(1,128)S(1)} all-gather(f32[1,1,2]{2,1,0:T(1,128)S(1)} %get-tuple-element.30), channel_id=1, replica_groups=mesh['sp_0'=4,'sp_1'=4,'sp_2'=4,'tp'=2] {'sp_0'}, dimensions={0}, use_global_device_ids=true | all-gather | bytes 40 | tf_op jit(solution)/shard_map/all_gather | solution.py:41
  99.9 0.4 fusion.2
  100.3 22.9 %all-gather.12.cloned.1.call-done = f32[4,8,2,64,128]{4,3,2,1,0:T(8,128)} async-done(((f32[1,8,2,64,128]{4,3,2,1,0:T(8,128)}), f32[4,8,2,64,128]{4,3,2,1,0:T(8,128)}) %all-gather.12.cloned.1.call-update) | async-done | bytes 2097168 | tf_op jit(solution)/shard_map/all_gather | solution.py:41
  123.2 4.4 %fusion.120 = (f32[8,64,2]{1,2,0:T(2,128)S(1)}, f32[8,64,2,128]{3,1,2,0:T(8,128)S(1)}) fusion(f32[8,2,128,64]{2,3,1,0:T(8,128)S(1)} %fusion.2, f32[64,2]{0,1:T(2,128)S(1)} %get-tuple-element.40, bf16[8,64,2,32]{3,1,2,0:T(8,128)(2,1)S(1)} %get-tuple-element.12, bf16[8,64,2,32]{3,1,2,0:T(8,128)(2,1)S(1)} %get-tuple-element.11, ...), kind=kOutput, calls=%fused_computation.197 | convolution fusion | flops 106363904 | bytes 8000132 | tf_op jit(solution)/shard_map/schd,shde->sche/dot_general | solution.py:149
  128.5 1.5 convolution_convert_fusion
  130.0 101.7 %all-reduce.2.cloned.1.call-done = f32[8,2,64,128]{3,2,1,0:T(8,128)} async-done(((f32[8,2,64,128]{3,2,1,0:T(8,128)}), f32[8,2,64,128]{3,2,1,0:T(8,128)}) %all-reduce.2.cloned.1.call-update) | async-done | bytes 524304 | tf_op jit(solution)/shard_map/psum | solution.py:171
  231.6 2.0 multiply_add_fusion
  233.6 2.1 copy.35
  (57 shorter events, 3.0 us)
Async XLA Ops:
  8.0 120.5 %copy-start = (bf16[256,1024]{1,0:T(8,128)(2,1)S(1)}, bf16[256,1024]{1,0:T(8,128)(2,1)}, u32[]{:S(2)}) copy-start(bf16[256,1024]{1,0:T(8,128)(2,1)} %param.16) | copy-start | bytes 1572868
  8.0 47.1 %all-gather.14.cloned.1.call-start = ((), (), s32[]{:S(2)}) async-start(), calls=%async_computation.5 | async-start | bytes 2621440 | tf_op jit(solution)/shard_map/all_gather | solution.py:41
  8.8 8.0 %copy-start.2 = (bf16[1024,256]{1,0:T(8,128)(2,1)S(1)}, bf16[1024,256]{1,0:T(8,128)(2,1)}, u32[]{:S(2)}) copy-start(bf16[1024,256]{1,0:T(8,128)(2,1)} %param.14) | copy-start | bytes 1572868
  8.8 8.0 %copy-start.3 = (bf16[1024,256]{1,0:T(8,128)(2,1)S(1)}, bf16[1024,256]{1,0:T(8,128)(2,1)}, u32[]{:S(2)}) copy-start(bf16[1024,256]{1,0:T(8,128)(2,1)} %param.13) | copy-start | bytes 1572868
  8.8 8.0 %copy-start.4 = (bf16[1024,128]{1,0:T(8,128)(2,1)S(1)}, bf16[1024,128]{1,0:T(8,128)(2,1)}, u32[]{:S(2)}) copy-start(bf16[1024,128]{1,0:T(8,128)(2,1)} %param.12) | copy-start | bytes 786436
  8.8 8.0 %copy-start.5 = (bf16[1024,128]{1,0:T(8,128)(2,1)S(1)}, bf16[1024,128]{1,0:T(8,128)(2,1)}, u32[]{:S(2)}) copy-start(bf16[1024,128]{1,0:T(8,128)(2,1)} %param.11) | copy-start | bytes 786436
  22.3 66.2 %all-gather.10.cloned.1.call-start = ((), (), s32[]{:S(2)}) async-start(), calls=%async_computation.1 | async-start | bytes 2621440 | tf_op jit(solution)/shard_map/all_gather | solution.py:41
  57.6 42.1 %copy-start.6 = (bf16[2,128]{1,0:T(2,128)(2,1)S(1)}, bf16[2,128]{1,0:T(2,128)(2,1)}, u32[]{:S(2)}) copy-start(bf16[2,128]{1,0:T(2,128)(2,1)} %param.15) | copy-start | bytes 1540
  57.7 65.6 %all-gather.12.cloned.1.call-start = ((), (), s32[]{:S(2)}) async-start(), calls=%async_computation.2 | async-start | bytes 2621440 | tf_op jit(solution)/shard_map/all_gather | solution.py:41
  91.1 32.1 %copy-start.1 = (f32[8,2,64,128]{3,2,1,0:T(8,128)S(1)}, f32[8,2,64,128]{3,2,1,0:T(8,128)}, u32[]{:S(2)}) copy-start(f32[8,2,64,128]{3,2,1,0:T(8,128)} %param.17) | copy-start | bytes 1572868
  91.1 140.5 %all-reduce.2.cloned.1.call-start = ((), (), s32[]{:S(2)}) async-start(), calls=%async_computation.4 | async-start | bytes 1048576 | tf_op jit(solution)/shard_map/psum | solution.py:171
  91.7 141.9 %reduce-scatter.2.cloned.1.call-start = ((), (), s32[]{:S(2)}) async-start(), calls=%async_computation.3 | async-start | bytes 1572864 | tf_op jit(solution)/shard_map/reduce_scatter | solution.py:53
Sparse Core Ops, SparseCore 0:
  22.4 32.5 all-gather.13
  57.8 30.7 all-gather.9
  91.3 31.9 all-gather.11
  130.1 11.8 reduce-scatter.1
Sparse Core Ops, SparseCore 1:
  96.9 134.6 all-reduce.1
where the time goes:
time: 245 us; the launch traced here: 243 us
  waiting for transfers between devices  173 us (71%)
  blocking collectives  28.8 us (12%)
  between operations  15.5 us (6%)
  other arithmetic  12.4 us (5%)
  matrix products  8.82 us (4%)
  local copies, waits for them, and re-layouts  4.07 us (2%)
    psum x1, waiting for transfers between devices, per_device(): total = lax.psum(local_state * factor[None, :, None, None], SP)  102 us
    all_gather x3, waiting for transfers between devices, entering(): pieces = jax.tree.map(lambda part: lax.all_gather(part, axis), so_far)  70.8 us
    all_gather x3, blocking collectives, entering(): pieces = jax.tree.map(lambda part: lax.all_gather(part, axis), so_far)  23.5 us
    all_gather x2, blocking collectives, on_gathered_pieces(): parts = [lax.all_gather(slab, axis) for slab in pieces]  5.34 us
    add x2, other arithmetic, combine(): earlier[1] * later[0][None, :, None, None] + later[1]  5.12 us
  transfers between devices with their start and end apart: 5, of which 4 were waited for; matrix products, arithmetic and copies ran while one was open for 4% of the time, Pallas kernels for 0%

commit v1 on v0

v1 whole, which is shorter than its diff:
```python
import functools

import jax
import jax.numpy as jnp
import numpy as np
from jax import lax
from jax.experimental import pallas as pl
from jax.experimental.pallas import tpu as pltpu
from jax.sharding import Mesh
from jax.sharding import PartitionSpec as P

SP = ("sp_0", "sp_1", "sp_2")
SP_TP = ("sp_0", "sp_1", "sp_2", "tp")
MESH = pl.DeviceIdType.MESH

EPS = 1e-06
ROPE_BASE = 10000.0

SEQS, HALF, D = 8, 32, 1024
STRETCH = 2 * HALF
BLOCKS = 64
DK, DV = 64, 128
KEYS, VALS = 2 * DK, 2 * DV
TILE = 16
F32, BF16 = jnp.float32, jnp.bfloat16


def tables():
    lane = np.arange(KEYS)
    freqs = ROPE_BASE ** (-2.0 * (lane % 32) / DK)
    sign = np.where(lane % DK < 32, -1.0, 1.0)
    start = (np.arange(BLOCKS) * STRETCH)[:, None] * freqs
    step = np.arange(STRETCH)[:, None] * freqs
    base = np.zeros((BLOCKS, 8, KEYS))
    base[:, 0], base[:, 1], base[:, 2] = np.cos(start), np.sin(start), sign * np.sin(start)
    turn = np.stack([np.cos(step), np.sin(step), sign * np.sin(step)])
    lg = -(0.25 + 0.25 * np.arange(4)) / (BLOCKS * STRETCH)
    pos = np.arange(STRETCH)
    decay = np.zeros((2, 208, KEYS))
    mask = np.zeros((2, 4, STRETCH, 2, STRETCH))
    gap = pos[:, None] - pos[None, :]
    for t in range(2):
        for h in range(2):
            g = lg[2 * t + h]
            decay[t, :64, h * DK : (h + 1) * DK] = np.exp((STRETCH - 1 - pos) * g)[:, None]
            decay[t, 64 + 64 * h : 128 + 64 * h] = np.exp((pos + 1) * g)[:, None]
            decay[t, 192 + 8 * h : 200 + 8 * h] = np.exp(STRETCH * g)
            for s in range(2):
                mask[t, 2 * h + s, :, s] = np.where(gap >= 0, np.exp(np.maximum(gap, 0) * g), 0)
    mask = mask.reshape(2, 4 * STRETCH, 2 * STRETCH)
    return [np.asarray(a, np.float32) for a in (base, turn, decay, mask)]


def dot(a, b):
    return jnp.dot(a, b, preferred_element_type=F32)


def layer(
    x_hbm, gain_hbm, wq_hbm, wk_hbm, wv_hbm, wg_hbm, hg_hbm, wo_hbm, init_hbm,
    base_hbm, turn_hbm, decay_hbm, mask_hbm,
    out_hbm, close_hbm,
    x_own, x_oth, gain, w_in, w_own, w_oth, hgain, init, base, turn, decay, mask,
    normed, cosine, sine, keys, wkeys, values, queries, gate, inner,
    send1, recv1, send2, incoming, csend, closing, mix, mix_oth, out, close,
    load_sem, store_sem, xs_sem, xr_sem, a_send, a_recv, sem2, sem3,
):
    z, y, x, t = (lax.axis_index(a) for a in SP_TP)
    me = (z * 4 + y) * 4 + x

    piece = me // 4
    loads = [
        pltpu.make_async_copy(src, dst, load_sem.at[k])
        for k, (src, dst) in enumerate(
            (
                (x_hbm, x_own),
                (gain_hbm, gain),
                (wk_hbm, w_in.at[:, pl.ds(0, KEYS)]),
                (wv_hbm, w_in.at[:, pl.ds(KEYS, VALS)]),
                (base_hbm.at[me], base),
                (turn_hbm, turn),
                (decay_hbm.at[t], decay),
                (wq_hbm, w_in.at[:, pl.ds(KEYS + VALS, KEYS)]),
                (wg_hbm, w_in.at[:, pl.ds(2 * KEYS + VALS, VALS)]),
                (hg_hbm, hgain),
                (mask_hbm.at[t], mask),
                (init_hbm.at[piece // 2, lax.rem(piece, 2), pl.ds(TILE * lax.rem(me, 4), TILE)], init),
                (wo_hbm, w_own),
            )
        )
    ]
    partner = (z, y, x, 1 - t)
    barrier = pltpu.get_barrier_semaphore()
    for k in (1, 2, 3):
        for there in (
            (lax.rem(z + k, 4), y, x, t),
            (z, lax.rem(y + k, 4), x, t),
            (z, y, lax.rem(x + k, 4), t),
        ):
            pl.semaphore_signal(barrier, inc=1, device_id=there, device_id_type=MESH)
    pl.semaphore_signal(barrier, inc=1, device_id=partner, device_id_type=MESH)
    for copy in loads:
        copy.start()

    loads[0].wait()
    pl.semaphore_wait(barrier, 10)
    swap_x = pltpu.make_async_remote_copy(
        src_ref=x_own, dst_ref=x_oth, send_sem=xs_sem.at[0], recv_sem=xr_sem.at[0],
        device_id=partner, device_id_type=MESH,
    )
    swap_x.start()
    for k in (1, 2, 3):
        pl.semaphore_signal(sem2, inc=1, device_id=(z, lax.rem(y + k, 4), x, t), device_id_type=MESH)

    for k in range(1, 7):
        loads[k].wait()
    cosine[...] = base[0:1, :] * turn[0] - base[1:2, :] * turn[1]
    sine[...] = base[2:3, :] * turn[0] + base[0:1, :] * turn[2]

    lane = lax.broadcasted_iota(jnp.int32, (1, 1, KEYS), 2)
    low = lax.rem(lane, DK) < DK // 2
    gains = gain[...].astype(F32)

    def norm(x_ref):
        def rows(s, carry):
            f = x_ref[s].astype(F32)
            ms = jnp.mean(f * f, axis=-1, keepdims=True)
            normed[pl.ds(pl.multiple_of(s * HALF, HALF), HALF), :] = (
                f * lax.rsqrt(ms + EPS) * gains
            ).astype(BF16)
            return carry

        lax.fori_loop(0, SEQS, rows, 0)

    def rotary(p, row):
        v = p.reshape(SEQS, HALF, KEYS)
        flat = p
        other = jnp.where(
            low, pltpu.roll(flat, KEYS - 32, 1).reshape(v.shape), pltpu.roll(flat, 32, 1).reshape(v.shape)
        )
        return v * cosine[pl.ds(row, HALF), :][None] + other * sine[pl.ds(row, HALF), :][None]

    def keys_values(row):
        p = dot(normed[...], w_in[:, : KEYS + VALS])
        values[:, pl.ds(row, HALF), :] = p[:, KEYS:].astype(BF16).reshape(SEQS, HALF, VALS)
        k = (rotary(p[:, :KEYS].astype(BF16).astype(F32), row) * DK**-0.5).astype(BF16)
        keys[:, pl.ds(row, HALF), :] = k
        wkeys[:, pl.ds(row, HALF), :] = (k.astype(F32) * decay[pl.ds(row, HALF), :][None]).astype(BF16)

    def queries_gates(row):
        p = dot(normed[...], w_in[:, KEYS + VALS :])
        queries[:, pl.ds(row, HALF), :] = rotary(p[:, :KEYS].astype(BF16).astype(F32), row).astype(BF16)
        g = p[:, KEYS:].astype(BF16).astype(F32)
        gate[:, pl.ds(row, HALF), :] = jax.nn.silu(g).reshape(SEQS, HALF, VALS)

    row_own = pl.multiple_of(HALF * t, HALF)
    row_oth = pl.multiple_of(HALF * (1 - t), HALF)
    norm(x_own)
    keys_values(row_own)
    pl.semaphore_wait(sem2, 3)
    for k in (1, 2, 3):
        pl.semaphore_signal(sem3, inc=1, device_id=(lax.rem(z + k, 4), y, x, t), device_id_type=MESH)
    for k in range(7, 13):
        loads[k].wait()
    queries_gates(row_own)
    swap_x.wait()
    swap_w = pltpu.make_async_remote_copy(
        src_ref=w_own, dst_ref=w_oth, send_sem=xs_sem.at[1], recv_sem=xr_sem.at[1],
        device_id=partner, device_id_type=MESH,
    )
    swap_w.start()
    norm(x_oth)
    keys_values(row_oth)

    for s in range(SEQS):
        both = dot(wkeys[s].T, values[s])
        for h in range(2):
            part = both[h * DK : (h + 1) * DK, h * DV : (h + 1) * DV].astype(BF16)
            send1[pl.ds((2 * s + h) * 4, 4)] = part.reshape(4, TILE, DV)
    pl.semaphore_wait(sem3, 3)

    def to_all(source, landing, k_sem):
        def one(k, carry):
            there = lax.rem(me + k, BLOCKS)
            pltpu.make_async_remote_copy(
                src_ref=source(there), dst_ref=landing.at[me],
                send_sem=a_send.at[k_sem], recv_sem=a_recv.at[k_sem],
                device_id=(there // 16, lax.rem(there // 4, 4), lax.rem(there, 4), t),
                device_id_type=MESH,
            ).start()
            return carry

        lax.fori_loop(1, BLOCKS, one, 0)

    def await_all(buffer, sem):
        rest = buffer.at[pl.ds(0, BLOCKS - 1)]
        pltpu.make_async_copy(rest, rest, sem).wait()

    to_all(lambda there: send1.at[there], recv1, 0)
    recv1[me] = send1[me]

    queries_gates(row_oth)
    first = lax.broadcasted_iota(jnp.int32, (1, KEYS), 1) < DK
    for j in range(SEQS // 2):
        q = queries[2 * j : 2 * j + 2].reshape(2 * STRETCH, KEYS)
        zero = jnp.zeros_like(q)
        stacked = jnp.concatenate([jnp.where(first, q, zero), jnp.where(first, zero, q)], axis=0)
        k = keys[2 * j : 2 * j + 2].reshape(2 * STRETCH, KEYS)
        scores = lax.dot_general(stacked, k, (((1,), (1,)), ((), ())), preferred_element_type=F32)
        scores = (scores * mask[...]).astype(BF16)
        v = values[2 * j : 2 * j + 2].reshape(2 * STRETCH, VALS)
        for h in range(2):
            cols = slice(h * DV, (h + 1) * DV)
            got = dot(scores[h * 2 * STRETCH : (h + 1) * 2 * STRETCH], v[:, cols])
            inner[2 * j : 2 * j + 2, :, cols] = got.reshape(2, STRETCH, DV)

    block_decay = decay[pl.ds(pl.multiple_of(192 + 8 * lax.rem(piece, 2), 8), 8), :]
    block_decay = jnp.concatenate([block_decay, block_decay], axis=0)
    await_all(recv1, a_recv.at[0])
    state = init[...]
    for j in range(BLOCKS):
        send2[j] = state.astype(BF16)
        state = state * block_decay + recv1[j].astype(F32)
    csend[...] = state.astype(BF16)
    to_all(lambda there: send2.at[there], incoming, 1)
    to_all(lambda there: csend, closing, 2)
    incoming[me] = send2[me]
    closing[me] = csend[...]
    await_all(incoming, a_recv.at[1])

    gains_h = hgain[...].astype(F32)
    for s in range(SEQS):
        q = queries[s]
        s0 = incoming[pl.ds(8 * s, 4)].reshape(DK, DV)
        s1 = incoming[pl.ds(8 * s + 4, 4)].reshape(DK, DV)
        zero = jnp.zeros_like(s0)
        cross = dot(q, jnp.concatenate(
            [jnp.concatenate([s0, zero], axis=1), jnp.concatenate([zero, s1], axis=1)], axis=0
        ))
        for h in range(2):
            cols = slice(h * DV, (h + 1) * DV)
            kept = inner[s, :, cols] + cross[:, cols] * decay[64 + 64 * h : 128 + 64 * h, :]
            kept = kept - jnp.mean(kept, axis=-1, keepdims=True)
            spread = jnp.mean(kept * kept, axis=-1, keepdims=True)
            m = gate[s, :, cols] * (kept * lax.rsqrt(spread + EPS) * gains_h[h : h + 1, :])
            m = m.astype(BF16)
            mix[0, s, :, cols] = m[:HALF]
            mix[1, s, :, cols] = m[HALF:]
    swap_m = pltpu.make_async_remote_copy(
        src_ref=mix.at[1 - t], dst_ref=mix_oth, send_sem=xs_sem.at[2], recv_sem=xr_sem.at[2],
        device_id=partner, device_id_type=MESH,
    )
    swap_m.start()
    part = dot(mix[t].reshape(SEQS * HALF, VALS), w_own[...])
    swap_w.wait()
    swap_m.wait()
    part = part + dot(mix_oth[...].reshape(SEQS * HALF, VALS), w_oth[...])
    out[...] = part.astype(BF16).reshape(SEQS, HALF, D)
    store = pltpu.make_async_copy(out, out_hbm, store_sem.at[0])
    store.start()
    await_all(closing, a_recv.at[2])
    close[...] = closing[...].astype(F32).reshape(SEQS, 2, DK, DV)
    store_c = pltpu.make_async_copy(close, close_hbm, store_sem.at[1])
    store_c.start()
    await_all(send1, a_send.at[0])
    await_all(send2, a_send.at[1])
    await_all(closing, a_send.at[2])
    store.wait()
    store_c.wait()


def per_device(x, norm_gain, w_query, w_key, w_value, w_gate, head_gain, w_out, initial_state):
    any_space = pl.BlockSpec(memory_space=pl.ANY)
    vmem = pltpu.VMEM
    dma = pltpu.SemaphoreType.DMA
    rows = (SEQS, STRETCH)
    args = (
        x, norm_gain.reshape(1, D), w_query, w_key, w_value, w_gate, head_gain, w_out, initial_state,
        *[jnp.asarray(a) for a in tables()],
    )
    return pl.pallas_call(
        layer,
        out_shape=(
            jax.ShapeDtypeStruct(x.shape, BF16),
            jax.ShapeDtypeStruct(initial_state.shape, F32),
        ),
        in_specs=[any_space] * len(args),
        out_specs=(any_space, any_space),
        scratch_shapes=[
            vmem((SEQS, HALF, D), BF16),
            vmem((SEQS, HALF, D), BF16),
            vmem((1, D), BF16),
            vmem((D, 2 * (KEYS + VALS)), BF16),
            vmem((VALS, D), BF16),
            vmem((VALS, D), BF16),
            vmem((2, DV), BF16),
            vmem((TILE, DV), F32),
            vmem((8, KEYS), F32),
            vmem((3, STRETCH, KEYS), F32),
            vmem((208, KEYS), F32),
            vmem((4 * STRETCH, 2 * STRETCH), F32),
            vmem((SEQS * HALF, D), BF16),
            vmem((STRETCH, KEYS), F32),
            vmem((STRETCH, KEYS), F32),
            vmem(rows + (KEYS,), BF16),
            vmem(rows + (KEYS,), BF16),
            vmem(rows + (VALS,), BF16),
            vmem(rows + (KEYS,), BF16),
            vmem(rows + (VALS,), F32),
            vmem(rows + (VALS,), F32),
            vmem((BLOCKS, TILE, DV), BF16),
            vmem((BLOCKS, TILE, DV), BF16),
            vmem((BLOCKS, TILE, DV), BF16),
            vmem((BLOCKS, TILE, DV), BF16),
            vmem((TILE, DV), BF16),
            vmem((BLOCKS, TILE, DV), BF16),
            vmem((2, SEQS, HALF, VALS), BF16),
            vmem((SEQS, HALF, VALS), BF16),
            vmem((SEQS, HALF, D), BF16),
            vmem((SEQS, 2, DK, DV), F32),
            dma((13,)), dma((2,)), dma((3,)), dma((3,)), dma((3,)), dma((3,)),
            pltpu.SemaphoreType.REGULAR, pltpu.SemaphoreType.REGULAR,
        ],
        compiler_params=pltpu.CompilerParams(collective_id=0, has_side_effects=True),
    )(*args)


def solution(mesh):
    split = Mesh(mesh.devices.reshape(4, 4, 4, mesh.shape["tp"]), SP_TP)
    placed = (
        P(None, SP_TP, None),
        P(),
        P(None, "tp"),
        P(None, "tp"),
        P(None, "tp"),
        P(None, "tp"),
        P("tp", None),
        P("tp", None),
        P(None, "tp", None, None),
    )
    return jax.shard_map(
        per_device,
        mesh=split,
        in_specs=placed,
        out_specs=(P(None, SP_TP, None), P(None, "tp", None, None)),
        check_vma=False,
    )
```

time: 245 us -> 33.9 us (0.14)
  waiting for transfers between devices: 173 us -> 0 us
  Pallas kernels: 0 us -> 29.1 us
  blocking collectives: 28.8 us -> 0 us
  between operations: 15.5 us -> 0.65 us
  other arithmetic: 12.4 us -> 0 us
  matrix products: 8.82 us -> 0 us
    psum x1 -> x0, waiting for transfers between devices: 102 us -> none  [per_device(): total = lax.psum(local_state * factor[None, :, None, None], SP)]
    all_gather x3 -> x0, waiting for transfers between devices: 70.8 us -> none  [entering(): pieces = jax.tree.map(lambda part: lax.all_gather(part, axis), so_far)]
    pallas_call x0 -> x1, Pallas kernels: none -> 29.1 us  [per_device(): pl.pallas_call(layer, out_shape=(jax.ShapeDtypeStruct(x.shape, BF16), jax...]
    all_gather x5 -> x0, blocking collectives: 28.8 us -> none  [the longest x3 23.5 us: entering(): pieces = jax.tree.map(lambda part: lax.all_gather(part, axis), so_far)]
    dot_general x6 -> x0, matrix products: 8.82 us -> none  [the longest x1 4.42 us: per_device(): jnp.einsum('schd,shde->sche', scaled_query, incoming, precision=lax.Preci...]
    add x4 -> x0, other arithmetic: 7.1 us -> none  [the longest x2 5.12 us: combine(): earlier[1] * later[0][None, :, None, None] + later[1]]
  transfers between devices with their start and end apart: 5 -> 0, of which waited for: 4 -> 0; matrix products, arithmetic and copies ran while one was open for 4% -> 0% of each run, Pallas kernels for 0% -> 0%
where the time goes in v1:
time: 33.9 us; the launch traced here: 33.7 us
  Pallas kernels  29.1 us (86%)
  local copies, waits for them, and re-layouts  4 us (12%)
  between operations  0.65 us (2%)
    pallas_call x1, Pallas kernels, per_device(): pl.pallas_call(layer, out_shape=(jax.ShapeDtypeStruct(x.shape, BF16), jax...  29.1 us
    unnamed x4, local copies, waits for them, and re-layouts  2.72 us
    reshape x1, local copies, waits for them, and re-layouts, per_device(): norm_gain.reshape(1, D)  1.28 us

profile of v1, /device:TPU:1, one launch (start us, length us, event | category | flops | bytes accessed | tf_op | source)
XLA Modules:
  0.0 33.7 jit_solution(3000570276649774782)
XLA Ops:
  0.6 1.3 %reshape.7.gain_hbm = bf16[1,1024]{1,0:T(2,128)(2,1)} reshape(bf16[1024]{0:T(1024)(128)(2,1)} %param.14) | data formatting | bytes 4096 | tf_op jit(solution)/shard_map/reshape | solution.py:277
  1.9 29.1 %shard_map.140 = (bf16[8,32,1024]{2,1,0:T(8,128)(2,1)}, f32[8,2,64,128]{3,2,1,0:T(8,128)}) custom-call(bf16[8,32,1024]{2,1,0:T(8,128)(2,1)} %x_hbm.1, bf16[1,1024]{1,0:T(2,128)(2,1)} %reshape.7.gain_hbm, bf16[1024,128]{1,0:T(8,128)(2,1)} %wq_hbm.1, bf16[1024,128]{1,0:T(8,128)(2,1)} %wk_hbm.1, bf16[1024,256]{1,0:T(8,128)(2,1)} %wv_hbm.1, ...), custom_call_target="tpu_custom_call" | custom-call | tf_op jit(solution)/shard_map/pallas_call | solution.py:280
  31.0 0.0 copy-start
  31.0 1.9 %copy.17 = bf16[8,32,1024]{2,1,0:T(8,128)(2,1)} copy(bf16[8,32,1024]{2,1,0:T(8,128)(2,1)} %get-tuple-element.4) | data formatting | bytes 1048576
  32.9 0.0 copy-done
  32.9 0.8 %copy.18 = f32[8,2,64,128]{3,2,1,0:T(8,128)} copy(f32[8,2,64,128]{3,2,1,0:T(8,128)S(1)} %copy-done) | data formatting | bytes 1048576
Async XLA Ops:
  31.0 1.9 %copy-start = (f32[8,2,64,128]{3,2,1,0:T(8,128)S(1)}, f32[8,2,64,128]{3,2,1,0:T(8,128)}, u32[]{:S(2)}) copy-start(f32[8,2,64,128]{3,2,1,0:T(8,128)} %get-tuple-element.5) | copy-start | bytes 1572868

commit v2 on v1

--- a/solution.py
+++ b/solution.py
@@ -23,6 +23,10 @@
 KEYS, VALS = 2 * DK, 2 * DV
 TILE = 16
 F32, BF16 = jnp.float32, jnp.bfloat16
+FAR_FIRST = sorted(
+    [(a, b, c) for a in range(4) for b in range(4) for c in range(4) if a or b or c],
+    key=lambda o: -sum(min(k, 4 - k) for k in o),
+)
 
 
 def tables():
@@ -58,11 +62,11 @@
 def layer(
     x_hbm, gain_hbm, wq_hbm, wk_hbm, wv_hbm, wg_hbm, hg_hbm, wo_hbm, init_hbm,
     base_hbm, turn_hbm, decay_hbm, mask_hbm,
-    out_hbm, close_hbm,
-    x_own, x_oth, gain, w_in, w_own, w_oth, hgain, init, base, turn, decay, mask,
+    mix, mix_oth, w_own, w_oth, closing,
+    x_own, x_oth, gain, w_in, hgain, init, base, turn, decay, mask,
     normed, cosine, sine, keys, wkeys, values, queries, gate, inner,
-    send1, recv1, send2, incoming, csend, closing, mix, mix_oth, out, close,
-    load_sem, store_sem, xs_sem, xr_sem, a_send, a_recv, sem2, sem3,
+    send1, recv1, send2, incoming, csend,
+    load_sem, xs_sem, xr_sem, a_send, a_recv, sem2, sem3,
 ):
     z, y, x, t = (lax.axis_index(a) for a in SP_TP)
     me = (z * 4 + y) * 4 + x
@@ -101,15 +105,15 @@
     for copy in loads:
         copy.start()
 
+    pl.semaphore_wait(barrier, 10)
+    for k in (1, 2, 3):
+        pl.semaphore_signal(sem2, inc=1, device_id=(z, lax.rem(y + k, 4), x, t), device_id_type=MESH)
     loads[0].wait()
-    pl.semaphore_wait(barrier, 10)
     swap_x = pltpu.make_async_remote_copy(
         src_ref=x_own, dst_ref=x_oth, send_sem=xs_sem.at[0], recv_sem=xr_sem.at[0],
         device_id=partner, device_id_type=MESH,
     )
     swap_x.start()
-    for k in (1, 2, 3):
-        pl.semaphore_signal(sem2, inc=1, device_id=(z, lax.rem(y + k, 4), x, t), device_id_type=MESH)
 
     for k in range(1, 7):
         loads[k].wait()
@@ -118,13 +122,13 @@
 
     lane = lax.broadcasted_iota(jnp.int32, (1, 1, KEYS), 2)
     low = lax.rem(lane, DK) < DK // 2
-    gains = gain[...].astype(F32)
-
-    def norm(x_ref):
+    gains = gain[...].astype(F32).reshape(1, D)
+
+    def norm(x_ref, side):
         def rows(s, carry):
             f = x_ref[s].astype(F32)
             ms = jnp.mean(f * f, axis=-1, keepdims=True)
-            normed[pl.ds(pl.multiple_of(s * HALF, HALF), HALF), :] = (
+            normed[side, pl.ds(pl.multiple_of(s * HALF, HALF), HALF), :] = (
                 f * lax.rsqrt(ms + EPS) * gains
             ).astype(BF16)
             return carry
@@ -139,37 +143,35 @@
         )
         return v * cosine[pl.ds(row, HALF), :][None] + other * sine[pl.ds(row, HALF), :][None]
 
-    def keys_values(row):
-        p = dot(normed[...], w_in[:, : KEYS + VALS])
+    def keys_values(side, row):
+        p = dot(normed[side], w_in[:, : KEYS + VALS])
         values[:, pl.ds(row, HALF), :] = p[:, KEYS:].astype(BF16).reshape(SEQS, HALF, VALS)
         k = (rotary(p[:, :KEYS].astype(BF16).astype(F32), row) * DK**-0.5).astype(BF16)
         keys[:, pl.ds(row, HALF), :] = k
         wkeys[:, pl.ds(row, HALF), :] = (k.astype(F32) * decay[pl.ds(row, HALF), :][None]).astype(BF16)
 
-    def queries_gates(row):
-        p = dot(normed[...], w_in[:, KEYS + VALS :])
+    def queries_gates(side, row):
+        p = dot(normed[side], w_in[:, KEYS + VALS :])
         queries[:, pl.ds(row, HALF), :] = rotary(p[:, :KEYS].astype(BF16).astype(F32), row).astype(BF16)
         g = p[:, KEYS:].astype(BF16).astype(F32)
         gate[:, pl.ds(row, HALF), :] = jax.nn.silu(g).reshape(SEQS, HALF, VALS)
 
     row_own = pl.multiple_of(HALF * t, HALF)
     row_oth = pl.multiple_of(HALF * (1 - t), HALF)
-    norm(x_own)
-    keys_values(row_own)
+    norm(x_own, 0)
     pl.semaphore_wait(sem2, 3)
     for k in (1, 2, 3):
         pl.semaphore_signal(sem3, inc=1, device_id=(lax.rem(z + k, 4), y, x, t), device_id_type=MESH)
-    for k in range(7, 13):
-        loads[k].wait()
-    queries_gates(row_own)
+    keys_values(0, row_own)
     swap_x.wait()
+    loads[12].wait()
     swap_w = pltpu.make_async_remote_copy(
         src_ref=w_own, dst_ref=w_oth, send_sem=xs_sem.at[1], recv_sem=xr_sem.at[1],
         device_id=partner, device_id_type=MESH,
     )
     swap_w.start()
-    norm(x_oth)
-    keys_values(row_oth)
+    norm(x_oth, 1)
+    keys_values(1, row_oth)
 
     for s in range(SEQS):
         both = dot(wkeys[s].T, values[s])
@@ -179,17 +181,14 @@
     pl.semaphore_wait(sem3, 3)
 
     def to_all(source, landing, k_sem):
-        def one(k, carry):
-            there = lax.rem(me + k, BLOCKS)
+        zs, ys, xs = ([lax.rem(a + k, 4) for k in range(4)] for a in (z, y, x))
+        for kz, ky, kx in FAR_FIRST:
+            there = (zs[kz] * 4 + ys[ky]) * 4 + xs[kx]
             pltpu.make_async_remote_copy(
                 src_ref=source(there), dst_ref=landing.at[me],
                 send_sem=a_send.at[k_sem], recv_sem=a_recv.at[k_sem],
-                device_id=(there // 16, lax.rem(there // 4, 4), lax.rem(there, 4), t),
-                device_id_type=MESH,
+                device_id=(zs[kz], ys[ky], xs[kx], t), device_id_type=MESH,
             ).start()
-            return carry
-
-        lax.fori_loop(1, BLOCKS, one, 0)
 
     def await_all(buffer, sem):
         rest = buffer.at[pl.ds(0, BLOCKS - 1)]
@@ -198,7 +197,20 @@
     to_all(lambda there: send1.at[there], recv1, 0)
     recv1[me] = send1[me]
 
-    queries_gates(row_oth)
+    for k in range(7, 12):
+        loads[k].wait()
+    queries_gates(0, row_own)
+    queries_gates(1, row_oth)
+    block_decay = decay[pl.ds(pl.multiple_of(192 + 8 * lax.rem(piece, 2), 8), 8), :]
+    block_decay = jnp.concatenate([block_decay, block_decay], axis=0)
+    await_all(recv1, a_recv.at[0])
+    state = init[...]
+    for j in range(BLOCKS):
+        send2[j] = state.astype(BF16)
+        state = state * block_decay + recv1[j].astype(F32)
+    csend[...] = state.astype(BF16)
+    to_all(lambda there: send2.at[there], incoming, 1)
+    incoming[me] = send2[me]
     first = lax.broadcasted_iota(jnp.int32, (1, KEYS), 1) < DK
     for j in range(SEQS // 2):
         q = queries[2 * j : 2 * j + 2].reshape(2 * STRETCH, KEYS)
@@ -213,17 +225,7 @@
             got = dot(scores[h * 2 * STRETCH : (h + 1) * 2 * STRETCH], v[:, cols])
             inner[2 * j : 2 * j + 2, :, cols] = got.reshape(2, STRETCH, DV)
 
-    block_decay = decay[pl.ds(pl.multiple_of(192 + 8 * lax.rem(piece, 2), 8), 8), :]
-    block_decay = jnp.concatenate([block_decay, block_decay], axis=0)
-    await_all(recv1, a_recv.at[0])
-    state = init[...]
-    for j in range(BLOCKS):
-        send2[j] = state.astype(BF16)
-        state = state * block_decay + recv1[j].astype(F32)
-    csend[...] = state.astype(BF16)
-    to_all(lambda there: send2.at[there], incoming, 1)
     to_all(lambda there: csend, closing, 2)
-    incoming[me] = send2[me]
     closing[me] = csend[...]
     await_all(incoming, a_recv.at[1])
 
@@ -250,55 +252,63 @@
         device_id=partner, device_id_type=MESH,
     )
     swap_m.start()
-    part = dot(mix[t].reshape(SEQS * HALF, VALS), w_own[...])
-    swap_w.wait()
-    swap_m.wait()
-    part = part + dot(mix_oth[...].reshape(SEQS * HALF, VALS), w_oth[...])
-    out[...] = part.astype(BF16).reshape(SEQS, HALF, D)
-    store = pltpu.make_async_copy(out, out_hbm, store_sem.at[0])
-    store.start()
     await_all(closing, a_recv.at[2])
-    close[...] = closing[...].astype(F32).reshape(SEQS, 2, DK, DV)
-    store_c = pltpu.make_async_copy(close, close_hbm, store_sem.at[1])
-    store_c.start()
     await_all(send1, a_send.at[0])
     await_all(send2, a_send.at[1])
     await_all(closing, a_send.at[2])
-    store.wait()
-    store_c.wait()
+    swap_w.wait()
+    swap_m.wait()
+
+
+def project_out(mix, mix_oth, w_own, w_oth, closing, out_hbm, close_hbm, out, close, sem):
+    t = lax.axis_index("tp")
+    close[...] = closing[...].astype(F32).reshape(SEQS, 2, DK, DV)
+    stores = [pltpu.make_async_copy(close, close_hbm, sem.at[0])]
+    stores[0].start()
+    for k in range(SEQS // 2):
+        seqs = pl.ds(2 * k, 2)
+        part = dot(mix[t, seqs].reshape(2 * HALF, VALS), w_own[...])
+        part = part + dot(mix_oth[seqs].reshape(2 * HALF, VALS), w_oth[...])
+        out[seqs] = part.astype(BF16).reshape(2, HALF, D)
+        stores.append(pltpu.make_async_copy(out.at[seqs], out_hbm.at[seqs], sem.at[1 + k]))
+        stores[-1].start()
+    for store in stores:
+        store.wait()
 
 
 def per_device(x, norm_gain, w_query, w_key, w_value, w_gate, head_gain, w_out, initial_state):
     any_space = pl.BlockSpec(memory_space=pl.ANY)
     vmem = pltpu.VMEM
+    in_vmem = pl.BlockSpec(memory_space=vmem)
     dma = pltpu.SemaphoreType.DMA
     rows = (SEQS, STRETCH)
     args = (
-        x, norm_gain.reshape(1, D), w_query, w_key, w_value, w_gate, head_gain, w_out, initial_state,
+        x, norm_gain, w_query, w_key, w_value, w_gate, head_gain, w_out, initial_state,
         *[jnp.asarray(a) for a in tables()],
     )
-    return pl.pallas_call(
+    handed = pl.pallas_call(
         layer,
         out_shape=(
-            jax.ShapeDtypeStruct(x.shape, BF16),
-            jax.ShapeDtypeStruct(initial_state.shape, F32),
+            vmem((2, SEQS, HALF, VALS), BF16),
+            vmem((SEQS, HALF, VALS), BF16),
+            vmem((VALS, D), BF16),
+            vmem((VALS, D), BF16),
+            vmem((BLOCKS, TILE, DV), BF16),
         ),
         in_specs=[any_space] * len(args),
-        out_specs=(any_space, any_space),
+        out_specs=(in_vmem,) * 5,
         scratch_shapes=[
             vmem((SEQS, HALF, D), BF16),
             vmem((SEQS, HALF, D), BF16),
-            vmem((1, D), BF16),
+            vmem((D,), BF16),
             vmem((D, 2 * (KEYS + VALS)), BF16),
-            vmem((VALS, D), BF16),
-            vmem((VALS, D), BF16),
             vmem((2, DV), BF16),
             vmem((TILE, DV), F32),
             vmem((8, KEYS), F32),
             vmem((3, STRETCH, KEYS), F32),
             vmem((208, KEYS), F32),
             vmem((4 * STRETCH, 2 * STRETCH), F32),
-            vmem((SEQS * HALF, D), BF16),
+            vmem((2, SEQS * HALF, D), BF16),
             vmem((STRETCH, KEYS), F32),
             vmem((STRETCH, KEYS), F32),
             vmem(rows + (KEYS,), BF16),
@@ -312,16 +322,25 @@
             vmem((BLOCKS, TILE, DV), BF16),
             vmem((BLOCKS, TILE, DV), BF16),
             vmem((TILE, DV), BF16),
-            vmem((BLOCKS, TILE, DV), BF16),
-            vmem((2, SEQS, HALF, VALS), BF16),
-            vmem((SEQS, HALF, VALS), BF16),
-            vmem((SEQS, HALF, D), BF16),
-            vmem((SEQS, 2, DK, DV), F32),
-            dma((13,)), dma((2,)), dma((3,)), dma((3,)), dma((3,)), dma((3,)),
+            dma((13,)), dma((3,)), dma((3,)), dma((3,)), dma((3,)),
             pltpu.SemaphoreType.REGULAR, pltpu.SemaphoreType.REGULAR,
         ],
         compiler_params=pltpu.CompilerParams(collective_id=0, has_side_effects=True),
     )(*args)
+    return pl.pallas_call(
+        project_out,
+        out_shape=(
+            jax.ShapeDtypeStruct(x.shape, BF16),
+            jax.ShapeDtypeStruct(initial_state.shape, F32),
+        ),
+        in_specs=[in_vmem] * 5,
+        out_specs=(any_space, any_space),
+        scratch_shapes=[
+            vmem((SEQS, HALF, D), BF16),
+            vmem((SEQS, 2, DK, DV), F32),
+            dma((1 + SEQS // 2,)),
+        ],
+    )(*[pltpu.with_memory_space_constraint(a, vmem) for a in handed])
 
 
 def solution(mesh):

time: 33.9 us -> 29.1 us (0.86)
  local copies, waits for them, and re-layouts: 4 us -> 0 us
  Pallas kernels: 29.1 us -> 28.4 us
    unnamed x4 -> x0, local copies, waits for them, and re-layouts: 2.72 us -> none
    reshape x1 -> x0, local copies, waits for them, and re-layouts: 1.28 us -> none  [per_device(): norm_gain.reshape(1, D)]
    pallas_call x1 -> x2, Pallas kernels: 29.1 us -> 28.4 us  [the longest x1 26.8 us: per_device(): pl.pallas_call(layer, out_shape=(vmem((2, SEQS, HALF, VALS), BF16), vmem(...]
where the time goes in v2:
time: 29.1 us; the launch traced here: 29 us
  Pallas kernels  28.4 us (98%)
  between operations  0.64 us (2%)
    pallas_call x1, Pallas kernels, per_device(): pl.pallas_call(layer, out_shape=(vmem((2, SEQS, HALF, VALS), BF16), vmem(...  26.8 us
    pallas_call x1, Pallas kernels, per_device(): pl.pallas_call(project_out, out_shape=(jax.ShapeDtypeStruct(x.shape, BF16...  1.56 us

profile of v2, /device:TPU:1, one launch (start us, length us, event | category | flops | bytes accessed | tf_op | source)
XLA Modules:
  0.0 29.0 jit_solution(15147084236688067634)
XLA Ops:
  0.6 26.8 %shard_map.140 = (bf16[2,8,32,256]{3,2,1,0:T(8,128)(2,1)S(1)}, bf16[8,32,256]{2,1,0:T(8,128)(2,1)S(1)}, bf16[256,1024]{1,0:T(8,128)(2,1)S(1)}, bf16[256,1024]{1,0:T(8,128)(2,1)S(1)}, bf16[64,16,128]{2,1,0:T(8,128)(2,1)S(1)}) custom-call(bf16[8,32,1024]{2,1,0:T(8,128)(2,1)} %x_hbm.1, bf16[1024]{0:T(1024)(128)(2,1)} %gain_hbm.1, bf16[1024,128]{1,0:T(8,128)(2,1)} %wq_hbm.1, ...), custom_call_target="tpu_custom_call" | custom-call | tf_op jit(solution)/shard_map/pallas_call | solution.py:289
  27.5 1.6 %shard_map.141 = (bf16[8,32,1024]{2,1,0:T(8,128)(2,1)}, f32[8,2,64,128]{3,2,1,0:T(8,128)}) custom-call(bf16[2,8,32,256]{3,2,1,0:T(8,128)(2,1)S(1)} %get-tuple-element.7.mix, bf16[8,32,256]{2,1,0:T(8,128)(2,1)S(1)} %get-tuple-element.8.mix_oth, bf16[256,1024]{1,0:T(8,128)(2,1)S(1)} %get-tuple-element.9.w_own, bf16[256,1024]{1,0:T(8,128)(2,1)S(1)} %get-tuple-element.10.w_oth, ...), custom_call_target="tpu_custom_call" | custom-call | tf_op jit(solution)/shard_map/pallas_call | solution.py:330
